TPU v7x, 256 devices: a whole 4x4x8 slice. The times are simulated.
256 devices in a mesh: ep: 64 (over z, y, core), tp: 4 (over x).
Axes of the slice: x: 4, y: 4, z: 8, core: 2. Of those that a mesh axis runs over, the one named last changes fastest.
Arguments:
- c_gate: bfloat16 [16384, 1024], P('ep', 'tp'), may hold values from -6 to 6
- b_gate: bfloat16 [16384, 1024], P('ep', 'tp'), may hold values from -6 to 6
- values: bfloat16 [16384, 1024], P('ep', 'tp'), may hold values from -6 to 6
- conv_taps: float32 [3, 1024], P(None, 'tp'), may hold values from -3.5 to 3.5
- w_mix_out: bfloat16 [1024, 2048], P('tp'), may hold values from -0.1875 to 0.1875
- moe_in: bfloat16 [32768, 2048], P(('ep', 'tp')), may hold values from -6 to 6
- norm_gain: float32 [2048], replicated, may hold values from 0.1 to 1.9
- route_ids: int32 [32768, 2], P(('ep', 'tp')), may hold values from 0 to 63, all different within a row; in each aligned block of 128 rows (0 to 127, 128 to 255, ...) at most 5 rows name the same one
- route_weights: float32 [32768, 2], P(('ep', 'tp')), may hold values from 0.1 to 1
- w_gate: bfloat16 [64, 2048, 3584], P('ep', None, 'tp'), may hold values from -0.125 to 0.125
- w_up: bfloat16 [64, 2048, 3584], P('ep', None, 'tp'), may hold values from -0.125 to 0.125
- w_down: bfloat16 [64, 3584, 2048], P('ep', 'tp'), may hold values from -0.09375 to 0.09375
Outputs:
- mixer_out: bfloat16 [16384, 2048], P(('ep', 'tp'))
- moe_out: bfloat16 [32768, 2048], P(('ep', 'tp'))
Inputs may be any that keep to these rules, and one draw needn't show every extreme that they name: `route_ids`: each row names 2 different experts; in each aligned block of 128 rows (the rows of one device) no expert is named by more than 5 rows, and in every draw some expert is named by exactly 5 rows in some block.
All inputs are finite; a program needn't handle non-finite values.
Results may differ from a plain program's by a relative error of at most 0.012.
Values may be sent and summed in bfloat16 or wider, within the bound.
A program may use at most 128 MiB of HBM per device.

v0:
```python
import jax
import jax.numpy as jnp
from jax import lax
from jax.sharding import PartitionSpec as P

EPS = 1e-06


def passed_along(block, axis, distance):
    devices = range(lax.axis_size(axis))
    route = [(i - distance, i) for i in devices if i - distance in devices]
    return lax.ppermute(block, axis, route)


def split_up(shard, dim, length):
    before, after = (shard.shape[:dim], shard.shape[dim + 1 :])
    return jnp.moveaxis(shard.reshape(*before, length, -1, *after), dim, 0)


def sent_and_summed(shard, axis, dim):
    blocks = split_up(shard, dim, lax.axis_size(axis))
    arrived = lax.all_to_all(blocks, axis, split_axis=0, concat_axis=0, tiled=True)
    return arrived.astype(jnp.float32).sum(axis=0)


def rank_copies(route_block, experts):
    flat_ids = route_block.reshape(-1)
    onehot = (flat_ids[:, None] == jnp.arange(experts, dtype=jnp.int32)[None, :]).astype(jnp.int32)
    before = jnp.cumsum(onehot, axis=0) - onehot
    return (flat_ids, jnp.sum(before * onehot, axis=1))


def pack_rows(rows, slot_of, top, slot_count):
    copies = slot_of.shape[0]
    table = (
        jnp.full((slot_count,), copies, jnp.int32)
        .at[slot_of]
        .set(jnp.arange(copies, dtype=jnp.int32))
    )
    padded = jnp.concatenate([rows, jnp.zeros((1, rows.shape[1]), rows.dtype)], 0)
    return padded[table // top]


def on_device(
    c_gate,
    b_gate,
    values,
    conv_taps,
    w_mix_out,
    moe_in,
    norm_gain,
    route_ids,
    route_weights,
    w_gate,
    w_up,
    w_down,
):
    tokens = c_gate.shape[0]
    reach = conv_taps.shape[0] - 1
    product = c_gate.astype(jnp.float32) * values.astype(jnp.float32)
    previous = passed_along(product[tokens - reach :], "ep", 1)
    extended = jnp.concatenate([previous, product], 0)
    convolved = jnp.zeros_like(product)
    for offset in range(reach + 1):
        convolved = convolved + conv_taps[offset][None, :] * extended[offset : offset + tokens]
    mixed = (b_gate.astype(jnp.float32) * convolved).astype(jnp.bfloat16)
    piece = mixed
    mixer_out = sent_and_summed(
        jnp.dot(piece, w_mix_out, preferred_element_type=jnp.float32).astype(jnp.bfloat16), "tp", 0
    ).astype(jnp.bfloat16)
    rows_b = moe_in.shape[0]
    width = moe_in.shape[1]
    top = route_ids.shape[1]
    n_ep = lax.axis_size("ep")
    experts = w_gate.shape[0] * n_ep
    capacity = 5 * rows_b * top // (4 * experts)
    stream = moe_in.astype(jnp.float32)
    scale = lax.rsqrt(jnp.mean(stream * stream, axis=1, keepdims=True) + EPS)
    normed = (stream * scale * norm_gain[None, :]).astype(jnp.bfloat16)
    own_ids, own_ranks = rank_copies(route_ids, experts)
    own_slot = own_ids * capacity + own_ranks
    outgoing = pack_rows(normed, own_slot, top, experts * capacity).reshape(
        experts, capacity, width
    )
    arrived = lax.all_to_all(outgoing, "ep", split_axis=0, concat_axis=1, tiled=True).reshape(
        -1, width
    )
    piece = lax.all_gather(arrived, "tp", axis=0, tiled=True)
    gate_val = jnp.dot(piece, w_gate[0], preferred_element_type=jnp.float32)
    up_val = jnp.dot(piece, w_up[0], preferred_element_type=jnp.float32)
    hidden = (jax.nn.silu(gate_val) * up_val).astype(jnp.bfloat16)
    piece = hidden
    expert_out = sent_and_summed(
        jnp.dot(piece, w_down[0], preferred_element_type=jnp.float32).astype(jnp.bfloat16), "tp", 0
    ).astype(jnp.bfloat16)
    returned = lax.all_to_all(
        expert_out.reshape(n_ep, capacity, width), "ep", split_axis=0, concat_axis=0, tiled=True
    )
    picked = returned.reshape(-1, width)[own_slot].astype(jnp.float32).reshape(rows_b, top, width)
    moe_out = jnp.sum(picked * route_weights[:, :, None], axis=1).astype(jnp.bfloat16)
    return (mixer_out, moe_out)


def solution(mesh):
    return jax.shard_map(
        on_device,
        mesh=mesh,
        in_specs=(
            P("ep", "tp"),
            P("ep", "tp"),
            P("ep", "tp"),
            P(None, "tp"),
            P("tp", None),
            P(("ep", "tp"), None),
            P(),
            P(("ep", "tp"), None),
            P(("ep", "tp"), None),
            P("ep", None, "tp"),
            P("ep", None, "tp"),
            P("ep", "tp", None),
        ),
        out_specs=(P(("ep", "tp"), None), P(("ep", "tp"), None)),
        check_vma=False,
    )
```

profile of v0, /device:TPU:8, one launch (start us, length us, event | category | flops | bytes accessed | tf_op | source)
XLA Modules:
  0.0 333.2 jit_solution(17508996634302096302)
XLA Ops:
  7.2 0.9 copy.16
  8.2 0.1 eq.25
  8.4 0.7 broadcast_multiply_fusion
  9.1 0.6 reduce-window.6
  9.7 0.2 slice_reduce_fusion
  10.0 0.1 mul.107
  10.3 1.4 scatter_custom_fusion
  11.7 1.2 fusion.4
  13.0 1.2 fusion.6
  14.3 3.0 gather_fusion
  17.3 2.4 reshape.88
  19.7 63.2 %all_to_all.24 = bf16[64,5,2048]{2,1,0:T(8,128)(2,1)} all-to-all(bf16[64,5,2048]{2,1,0:T(8,128)(2,1)S(1)} %reshape.88), channel_id=1, replica_groups=mesh['ep'=64,'tp'=4] {'ep'}, dimensions={0} | all-to-all | bytes 2621440 | tf_op jit(solution)/shard_map/all_to_all | solution.py:85
  82.9 3.7 %reshape.89 = bf16[320,2048]{1,0:T(8,128)(2,1)} reshape(bf16[64,5,2048]{2,1,0:T(8,128)(2,1)} %all_to_all.24) | data formatting | bytes 2621440 | tf_op jit(solution)/shard_map/reshape | solution.py:85
  86.6 55.8 %all-gather.2.cloned.1.call-done = bf16[1280,2048]{1,0:T(8,128)(2,1)} async-done(((bf16[320,2048]{1,0:T(8,128)(2,1)}), bf16[1280,2048]{1,0:T(8,128)(2,1)}) %all-gather.2.cloned.1.call-update) | async-done | bytes 5242896 | tf_op jit(solution)/shard_map/all_gather | solution.py:88
  142.4 10.0 %fusion.2 = f32[1280,896]{1,0:T(8,128)} fusion(bf16[1280,2048]{1,0:T(8,128)(2,1)} %all-gather.2.cloned.1.call-done, bf16[1,2048,896]{2,1,0:T(8,128)(2,1)} %param.21), kind=kOutput, calls=%fused_computation.7 | convolution fusion | flops 4697620480 | bytes 13500416 | tf_op jit(solution)/shard_map/dot_general | solution.py:89
  152.4 17.5 %convolution_convert_fusion = bf16[1280,2048]{1,0:T(8,128)(2,1)} fusion(bf16[1,896,2048]{2,1,0:T(8,128)(2,1)} %param.23, f32[1280,896]{1,0:T(8,128)} %fusion.2, bf16[1280,2048]{1,0:T(8,128)(2,1)} %all-gather.2.cloned.1.call-done, bf16[1,2048,896]{2,1,0:T(8,128)(2,1)} %param.22), kind=kOutput, calls=%fused_computation.3 | convolution fusion | flops 9404743680 | bytes 22413312 | tf_op jit(solution)/shard_map/dot_general | solution.py:94
  169.9 5.2 %all-to-all-start.2 = ((bf16[4,320,2048]{2,1,0:T(8,128)(2,1)}), bf16[4,320,2048]{2,1,0:T(8,128)(2,1)}, u32[]{:S(2)}, u32[]{:S(2)}) async-start(bf16[4,320,2048]{2,1,0:T(8,128)(2,1)} %bitcast.47), calls=%async_computation.2 | async-start | bytes 10485760 | tf_op jit(solution)/shard_map/all_to_all | solution.py:22
  175.2 1.9 collective-permute-start
  177.2 3.0 collective-permute-done
  180.1 1.5 convolution_convert_fusion.1
  181.6 53.8 %all-to-all-done.2 = bf16[4,320,2048]{2,1,0:T(8,128)(2,1)} async-done(((bf16[4,320,2048]{2,1,0:T(8,128)(2,1)}), bf16[4,320,2048]{2,1,0:T(8,128)(2,1)}, u32[]{:S(2)}, u32[]{:S(2)}) %all-to-all-start.2) | async-done | bytes 5242912 | tf_op jit(solution)/shard_map/all_to_all | solution.py:22
  235.4 3.7 %all-to-all-start = ((bf16[4,64,2048]{2,1,0:T(8,128)(2,1)}), bf16[4,64,2048]{2,1,0:T(8,128)(2,1)S(1)}, u32[]{:S(2)}, u32[]{:S(2)}) async-start(bf16[4,64,2048]{2,1,0:T(8,128)(2,1)} %bitcast.3), calls=%async_computation | async-start | bytes 2097152 | tf_op jit(solution)/shard_map/all_to_all | solution.py:22
  239.1 3.6 %reduce_sum.57 = bf16[320,2048]{1,0:T(8,128)(2,1)S(1)} reduce(bf16[4,320,2048]{2,1,0:T(8,128)(2,1)} %all-to-all-done.2, bf16[]{:T(256)} %constant.18.clone.1), dimensions={0}, to_apply=%region_6.7 | reduce | flops 1966080 | bytes 6553602 | tf_op jit(solution)/shard_map/reduce_sum | solution.py:23
  242.7 1.6 reshape.91
  244.3 8.9 %all-to-all-done = bf16[4,64,2048]{2,1,0:T(8,128)(2,1)S(1)} async-done(((bf16[4,64,2048]{2,1,0:T(8,128)(2,1)}), bf16[4,64,2048]{2,1,0:T(8,128)(2,1)S(1)}, u32[]{:S(2)}, u32[]{:S(2)}) %all-to-all-start) | async-done | bytes 1048608 | tf_op jit(solution)/shard_map/all_to_all | solution.py:22
  253.2 10.7 %all-to-all-start.3 = ((bf16[64,5,2048]{2,1,0:T(8,128)(2,1)}), bf16[64,5,2048]{2,1,0:T(8,128)(2,1)}, u32[]{:S(2)}, u32[]{:S(2)}) async-start(bf16[64,5,2048]{2,1,0:T(8,128)(2,1)} %reshape.91), calls=%async_computation.3 | async-start | bytes 4194304 | tf_op jit(solution)/shard_map/all_to_all | solution.py:96
  264.1 0.9 reduce_sum.53
  265.0 50.1 %all-to-all-done.3 = bf16[64,5,2048]{2,1,0:T(8,128)(2,1)} async-done(((bf16[64,5,2048]{2,1,0:T(8,128)(2,1)}), bf16[64,5,2048]{2,1,0:T(8,128)(2,1)}, u32[]{:S(2)}, u32[]{:S(2)}) %all-to-all-start.3) | async-done | bytes 1310752 | tf_op jit(solution)/shard_map/all_to_all | solution.py:96
  315.1 2.6 reshape.92
  317.7 2.3 gather_fusion.1
  320.0 2.4 reshape.93
  322.4 3.9 %multiply_reduce_fusion = bf16[128,2048]{1,0:T(8,128)(2,1)} fusion(f32[128,2,2048]{2,1,0:T(2,128)S(1)} %reshape.93, f32[128,2]{1,0:T(8,128)S(1)} %copy.19), kind=kLoop, calls=%fused_computation.10 | loop fusion | flops 786432 | bytes 2622464 | tf_op jit(solution)/shard_map/reduce_sum | solution.py:100
  (31 shorter events, 0.7 us)
Async XLA Ops:
  7.2 173.0 %copy-start = (bf16[256,2048]{1,0:T(8,128)(2,1)S(1)}, bf16[256,2048]{1,0:T(8,128)(2,1)}, u32[]{:S(2)}) copy-start(bf16[256,2048]{1,0:T(8,128)(2,1)} %param.16) | copy-start | bytes 3145732
  7.2 135.2 %all-gather.2.cloned.1.call-start = ((), (), s32[]{:S(2)}) async-start(), calls=%async_computation.4 | async-start | bytes 6553600 | tf_op jit(solution)/shard_map/all_gather | solution.py:88
  169.9 5.3 %copy-start.2 = (bf16[256,256]{1,0:T(8,128)(2,1)S(1)}, bf16[256,256]{1,0:T(8,128)(2,1)}, u32[]{:S(2)}) copy-start(bf16[256,256]{1,0:T(8,128)(2,1)} %param.14) | copy-start | bytes 393220
  169.9 5.3 %copy-start.3 = (bf16[256,256]{1,0:T(8,128)(2,1)S(1)}, bf16[256,256]{1,0:T(8,128)(2,1)}, u32[]{:S(2)}) copy-start(bf16[256,256]{1,0:T(8,128)(2,1)} %param.12) | copy-start | bytes 393220
  169.9 7.2 %copy-start.4 = (f32[3,256]{1,0:T(4,128)S(1)}, f32[3,256]{1,0:T(4,128)}, u32[]{:S(2)}) copy-start(f32[3,256]{1,0:T(4,128)} %param.15) | copy-start | bytes 9220
  169.9 10.2 %copy-start.1 = (bf16[256,256]{1,0:T(8,128)(2,1)S(1)}, bf16[256,256]{1,0:T(8,128)(2,1)}, u32[]{:S(2)}) copy-start(bf16[256,256]{1,0:T(8,128)(2,1)} %param.13) | copy-start | bytes 393220
  169.9 65.4 %all-to-all-start.2 = ((bf16[4,320,2048]{2,1,0:T(8,128)(2,1)}), bf16[4,320,2048]{2,1,0:T(8,128)(2,1)}, u32[]{:S(2)}, u32[]{:S(2)}) async-start(bf16[4,320,2048]{2,1,0:T(8,128)(2,1)} %bitcast.47), calls=%async_computation.2 | async-start | bytes 10485760 | tf_op jit(solution)/shard_map/all_to_all | solution.py:22
  175.2 4.9 %collective-permute-start = (f32[2,256]{1,0:T(2,128)S(1)}, f32[2,256]{1,0:T(2,128)S(1)}, u32[]{:S(2)}, u32[]{:S(2)}) collective-permute-start(f32[2,256]{1,0:T(2,128)S(1)} %slice.36), channel_id=1, source_target_pairs={{0,4},{4,8},{8,12},{12,16},{16,20},{20,24},{24,28},{28,32},{32,36}... | collective-permute-start | bytes 6152 | tf_op jit(solution)/shard_map/ppermute | solution.py:12
  235.4 17.8 %all-to-all-start = ((bf16[4,64,2048]{2,1,0:T(8,128)(2,1)}), bf16[4,64,2048]{2,1,0:T(8,128)(2,1)S(1)}, u32[]{:S(2)}, u32[]{:S(2)}) async-start(bf16[4,64,2048]{2,1,0:T(8,128)(2,1)} %bitcast.3), calls=%async_computation | async-start | bytes 2097152 | tf_op jit(solution)/shard_map/all_to_all | solution.py:22
  242.7 21.3 %copy-start.5 = (f32[128,2]{0,1:T(2,128)S(1)}, f32[128,2]{0,1:T(2,128)}, u32[]{:S(2)}) copy-start(f32[128,2]{0,1:T(2,128)} %param.20) | copy-start | bytes 3076
  253.2 61.9 %all-to-all-start.3 = ((bf16[64,5,2048]{2,1,0:T(8,128)(2,1)}), bf16[64,5,2048]{2,1,0:T(8,128)(2,1)}, u32[]{:S(2)}, u32[]{:S(2)}) async-start(bf16[64,5,2048]{2,1,0:T(8,128)(2,1)} %reshape.91), calls=%async_computation.3 | async-start | bytes 4194304 | tf_op jit(solution)/shard_map/all_to_all | solution.py:96
Sparse Core Ops, SparseCore 0:
  86.7 55.6 all-gather.1
where the time goes:
time: 334 us; the launch traced here: 333 us
  waiting for transfers between devices  172 us (51%)
  blocking collectives  63.2 us (19%)
  matrix products  29 us (9%)
  starting transfers between devices  21.6 us (6%)
  local copies, waits for them, and re-layouts  21.1 us (6%)
  between operations  14.2 us (4%)
  other arithmetic  12.4 us (4%)
    all_to_all x1, blocking collectives, on_device(): lax.all_to_all(outgoing, 'ep', split_axis=0, concat_axis=1, tiled=True)  63.2 us
    all_to_all x2, waiting for transfers between devices, sent_and_summed(): lax.all_to_all(blocks, axis, split_axis=0, concat_axis=0, tiled=True)  62.6 us
    all_gather x1, waiting for transfers between devices, on_device(): piece = lax.all_gather(arrived, 'tp', axis=0, tiled=True)  55.8 us
    all_to_all x1, waiting for transfers between devices, on_device(): lax.all_to_all(expert_out.reshape(n_ep, capacity, width), 'ep', split_axi...  50.1 us
    dot_general x1, matrix products, on_device(): jnp.dot(piece, w_down[0], preferred_element_type=jnp.float32)  17.5 us
    all_to_all x1, starting transfers between devices, on_device(): lax.all_to_all(expert_out.reshape(n_ep, capacity, width), 'ep', split_axi...  10.7 us
    dot_general x1, matrix products, on_device(): gate_val = jnp.dot(piece, w_gate[0], preferred_element_type=jnp.float32)  9.98 us
    all_to_all x2, starting transfers between devices, sent_and_summed(): lax.all_to_all(blocks, axis, split_axis=0, concat_axis=0, tiled=True)  8.91 us
  transfers between devices with their start and end apart: 5, of which 5 were waited for; matrix products, arithmetic and copies ran while one was open for 2% of the time, Pallas kernels for 0%

commit v1 on v0

v1 whole, which is shorter than its diff:
```python
import functools

import jax
import jax.numpy as jnp
import numpy as np
from jax import lax
from jax.experimental import pallas as pl
from jax.experimental.pallas import tpu as pltpu
from jax.sharding import PartitionSpec as P

EPS = 1e-06
MESH = pl.DeviceIdType.MESH
F32 = jnp.float32
BF16 = jnp.bfloat16
CAP = 5
PAD = 8


class Plan:
    def __init__(self, n_ep, n_tp, width, hidden, rows, tokens, channels):
        self.G = int(round(n_ep**0.5))
        self.NZ = n_ep // self.G
        assert self.G * self.NZ == n_ep and self.G == self.NZ and n_tp == 4
        self.X = n_tp
        self.D, self.F, self.T = width, hidden, rows
        self.TA, self.C = tokens, channels
        self.CB = CAP * self.G
        self.R = self.CB * self.NZ
        self.GS = 2 if self.NZ >= 8 else 1
        self.NG = self.NZ // self.GS
        self.dz = [0]
        for step in range(1, self.NZ // 2 + 1):
            self.dz.append(step)
            if step != self.NZ - step:
                self.dz.append(-step)
        assert len(self.dz) == self.NZ

    def off(self, k, rel, jj=0):
        return ((k * self.X + rel) * self.GS + jj) * self.CB


def body(
    p,
    c_gate,
    b_gate,
    values,
    conv_taps,
    w_mix_hbm,
    moe_in,
    norm_gain,
    route_ids,
    route_weights,
    perm,
    w_gate_hbm,
    w_up_hbm,
    w_down_hbm,
    mixer_out,
    moe_out,
    w_mix,
    w_gate,
    w_up,
    w_down,
    product,
    halo,
    mixed,
    m_part,
    m_turn,
    m_minus,
    m_plus,
    normed,
    send_a,
    recv_a,
    send_b,
    gathered,
    hid,
    part,
    turn,
    s_minus,
    s_plus,
    out_b,
    ret_b,
    send_r,
    ret_a,
    w_sem,
    halo_sem,
    a_sem,
    b_sem,
    ag_sem,
    fw_sem,
    rs_sem,
    mx_sem,
    rb_sem,
    ra_sem,
):
    G, NZ, X, D, F, T, CB, R, GS, NG = p.G, p.NZ, p.X, p.D, p.F, p.T, p.CB, p.R, p.GS, p.NG
    ep, x = lax.axis_index("ep"), lax.axis_index("tp")
    z, g = ep // G, ep % G
    half = D // 2

    def at(zz, gg, xx):
        return {"ep": zz * G + gg, "tp": xx}

    right, left = at(z, g, (x + 1) % X), at(z, g, (x + X - 1) % X)
    after = {"ep": (ep + 1) % (G * NZ), "tp": x}
    before = {"ep": (ep + G * NZ - 1) % (G * NZ), "tp": x}
    plane = [at(z, (g + d) % G, x) for d in range(G)]
    plane_back = [at(z, (g + G - d) % G, x) for d in range(G)]
    line = [at((z + NZ + dz) % NZ, g, x) for dz in p.dz]
    line_back = [at((z + NZ - dz) % NZ, g, x) for dz in p.dz]

    barrier = pltpu.get_barrier_semaphore()
    peers = plane[1:] + line[1:] + [right, left, after, before]
    for peer in peers:
        pl.semaphore_signal(barrier, inc=1, device_id=peer, device_id_type=MESH)

    def load(src, dst, i):
        copy = pltpu.make_async_copy(src, dst, w_sem.at[i])
        copy.start()
        return copy

    loads = [
        load(w_mix_hbm, w_mix, 0),
        load(w_gate_hbm.at[0], w_gate, 1),
        load(w_up_hbm.at[0], w_up, 2),
        load(w_down_hbm.at[0], w_down, 3),
    ]
    pending = []

    def remote(src, dst, sems, i, peer):
        copy = pltpu.make_async_remote_copy(
            src_ref=src,
            dst_ref=dst,
            send_sem=sems.at[0, i],
            recv_sem=sems.at[1, i],
            device_id=peer,
            device_id_type=MESH,
        )
        pending.append(copy)
        return copy

    def start(*args):
        copy = remote(*args)
        copy.start()
        return copy

    tokens = p.TA
    product[8 : 8 + tokens, :] = c_gate[...].astype(F32) * values[...].astype(F32)

    stream = moe_in[...].astype(F32)
    scale = lax.rsqrt(jnp.mean(stream * stream, axis=1, keepdims=True) + EPS)
    normed[...] = (stream * scale * norm_gain[...]).astype(BF16)

    rows_i = lax.broadcasted_iota(jnp.int32, (T, T), 0)
    cols_i = lax.broadcasted_iota(jnp.int32, (T, T), 1)
    eye, earlier = rows_i == cols_i, cols_i < rows_i

    def as_row(col):
        return jnp.sum(jnp.where(eye, col.astype(F32), 0.0), axis=0, keepdims=True).astype(jnp.int32)

    ids = [route_ids[:, 0:1], route_ids[:, 1:2]]
    id_rows = [as_row(col) for col in ids]
    slots = []
    for col in ids:
        seen = jnp.zeros((T, 1), F32)
        for row in id_rows:
            seen = seen + jnp.sum(
                jnp.where(earlier & (col == row), 1.0, 0.0), axis=1, keepdims=True
            )
        rank = seen.astype(jnp.int32)
        to_g = (col & (G - 1)) - g
        to_g = jnp.where(to_g < 0, to_g + G, to_g)
        to_z = (col >> (G.bit_length() - 1)) - z
        to_z = jnp.where(to_z < 0, to_z + NZ, to_z)
        slot_z = jnp.where(
            to_z == 0, 0, jnp.where(to_z <= NZ // 2, 2 * to_z - 1, 2 * (NZ - to_z))
        )
        slots.append(to_g * CB + slot_z * CAP + rank)
    slot_rows = [as_row(col) for col in slots]
    slot_i = lax.broadcasted_iota(jnp.int32, (R, T), 0)
    pick = jnp.where((slot_i == slot_rows[0]) | (slot_i == slot_rows[1]), 1.0, 0.0).astype(BF16)
    wide = min(512, D)

    def pack(i, _):
        cols = pl.ds(pl.multiple_of(i * wide, wide), wide)
        packed = jnp.dot(pick, normed[:, cols], preferred_element_type=F32).astype(BF16)
        send_a[0:R, cols] = packed
        recv_a[0:CB, cols] = packed[0:CB]
        return 0

    lax.fori_loop(0, D // wide, pack, 0)

    pl.semaphore_wait(barrier, len(peers))

    halo_copy = start(product.at[pl.ds(tokens, 8)], halo, halo_sem, 0, after)
    a_copies = [
        start(send_a.at[pl.ds(d * CB, CB)], recv_a.at[pl.ds(d * CB, CB)], a_sem, d, plane[d])
        for d in range(1, G)
    ]

    def rs_start(src, rows, offs, dst_off, turn, minus, plus, c0, c1, sems, i):
        mid = (c0 + c1) // 2
        lo, hi = pl.ds(c0, mid - c0), pl.ds(mid, c1 - mid)
        o0, o1, o2, o3 = (pl.ds(o, rows) for o in offs)
        od = pl.ds(dst_off, rows)
        c = {}
        c["tl"] = start(src.at[o2, lo], turn.at[od, lo], sems, i, right)
        c["tr"] = start(src.at[o2, hi], turn.at[od, hi], sems, i + 1, left)
        c["mh"] = start(src.at[o1, hi], minus.at[od, hi], sems, i + 2, right)
        c["pl"] = start(src.at[o3, lo], plus.at[od, lo], sems, i + 3, left)

        def middle():
            c["tl"].wait_recv()
            src[o1, lo] = (src[o1, lo].astype(F32) + turn[od, lo].astype(F32)).astype(BF16)
            c["ml"] = start(src.at[o1, lo], minus.at[od, lo], sems, i + 4, right)
            c["tr"].wait_recv()
            src[o3, hi] = (src[o3, hi].astype(F32) + turn[od, hi].astype(F32)).astype(BF16)
            c["ph"] = start(src.at[o3, hi], plus.at[od, hi], sems, i + 5, left)

        def end():
            for name in ("mh", "pl", "ml", "ph"):
                c[name].wait_recv()
            cols = pl.ds(c0, c1 - c0)
            total = src[o0, cols].astype(F32) + minus[od, cols].astype(F32)
            return (total + plus[od, cols].astype(F32)).astype(BF16)

        return middle, end

    halo_copy.wait_recv()
    product[0:8, :] = jnp.where(ep == 0, 0.0, halo[...])
    convolved = jnp.zeros((tokens, p.C), F32)
    taps = conv_taps.shape[0]
    for k in range(taps):
        convolved = convolved + conv_taps[k : k + 1, :] * product[pl.ds(8 - taps + 1 + k, tokens), :]
    mixed[...] = (b_gate[...].astype(F32) * convolved).astype(BF16)
    loads[0].wait()
    m_rows = tokens // X
    for rel in range(X):
        own = pl.ds(pl.multiple_of(((x + rel) % X) * m_rows, m_rows), m_rows)
        m_part[pl.ds(rel * m_rows, m_rows), :] = jnp.dot(
            mixed[own, :], w_mix[...], preferred_element_type=F32
        ).astype(BF16)
    m_middle, m_end = rs_start(
        m_part, m_rows, [rel * m_rows for rel in range(X)], 0, m_turn, m_minus, m_plus, 0, D, mx_sem, 0
    )

    for copy in a_copies:
        copy.wait_recv()

    def turn_in(i, _):
        cols = pl.ds(pl.multiple_of(i * wide, wide), wide)
        moved = jnp.dot(perm[...], recv_a[0:R, cols], preferred_element_type=F32).astype(BF16)
        send_b[0:R, cols] = moved
        gathered[0:CB, cols] = moved[0:CB]
        return 0

    lax.fori_loop(0, D // wide, turn_in, 0)

    def where(j, rel):
        return pl.ds(p.off(j // GS, rel, j % GS), CB)

    b_copies = [None] + [
        start(send_b.at[pl.ds(j * CB, CB)], gathered.at[where(j, 0)], b_sem, j, line[j])
        for j in range(1, NZ)
    ]
    ag, fw = {}, {}

    def gather_out(j):
        if j:
            b_copies[j].wait_recv()
        ag[j] = (
            start(gathered.at[where(j, 0)], gathered.at[where(j, 3)], ag_sem, 2 * j, right),
            start(gathered.at[where(j, 0)], gathered.at[where(j, 1)], ag_sem, 2 * j + 1, left),
        )

    def gather_on(j):
        lo, hi = pl.ds(0, half), pl.ds(half, half)
        ag[j][0].wait_recv()
        to_right = start(gathered.at[where(j, 3), lo], gathered.at[where(j, 2), lo], fw_sem, 2 * j, right)
        ag[j][1].wait_recv()
        to_left = start(gathered.at[where(j, 1), hi], gathered.at[where(j, 2), hi], fw_sem, 2 * j + 1, left)
        fw[j] = (to_right, to_left)

    rows_k = X * GS * CB

    def compute(k):
        for j in range(k * GS, (k + 1) * GS):
            fw[j][0].wait_recv()
            fw[j][1].wait_recv()
        r0 = p.off(k, 0)

        def up(t, _):
            cols = pl.ds(pl.multiple_of(t * 128, 128), 128)
            pair = jnp.concatenate([w_gate[:, cols], w_up[:, cols]], axis=1)
            both = jnp.dot(gathered[r0 : r0 + rows_k, :], pair, preferred_element_type=F32)
            hid[:, cols] = (jax.nn.silu(both[:, :128]) * both[:, 128:]).astype(BF16)
            return 0

        lax.fori_loop(0, F // 128, up, 0)

        def down(n, _):
            cols = pl.ds(pl.multiple_of(n * wide, wide), wide)
            part[r0 : r0 + rows_k, cols] = jnp.dot(
                hid[...], w_down[:, cols], preferred_element_type=F32
            ).astype(BF16)
            return 0

        lax.fori_loop(0, D // wide, down, 0)

    rs = {}
    rb = {}

    def sum_start(k):
        rs[k] = rs_start(
            part, GS * CB, [p.off(k, rel) for rel in range(X)], k * GS * CB,
            turn, s_minus, s_plus, 0, D, rs_sem, 6 * k,
        )

    def sum_end(k):
        total = rs[k][1]()
        for jj in range(GS):
            j = k * GS + jj
            rows = pl.ds(j * CB, CB)
            block = total[jj * CB : (jj + 1) * CB]
            if j == 0:
                ret_b[rows, :] = block
            else:
                out_b[rows, :] = block
                rb[j] = start(out_b.at[rows], ret_b.at[rows], rb_sem, j, line_back[j])

    m_middle()
    for s in range(NZ):
        gather_out(s)
        if s >= 1:
            gather_on(s - 1)
        if s == GS:
            for copy in loads[1:]:
                copy.wait()
        if s > GS and (s - 1) % GS == 0:
            compute((s - 1) // GS - 1)
        if s == NZ - 1:
            mixer_out[...] = m_end()
    gather_on(NZ - 1)
    order = list(range(NG // 2, NG)) + list(range(NG // 2 - 1, -1, -1))
    sum_start(order[0])
    compute(NG - 1)
    for i in range(NG + 1):
        if i + 1 < NG:
            sum_start(order[i + 1])
        if i < NG:
            rs[order[i]][0]()
        if i >= 1:
            sum_end(order[i - 1])

    for j in range(1, NZ):
        rb[j].wait_recv()

    def turn_out(i, _):
        cols = pl.ds(pl.multiple_of(i * wide, wide), wide)
        moved = jnp.dot(perm[...], ret_b[0:R, cols], preferred_element_type=F32).astype(BF16)
        send_r[0:R, cols] = moved
        ret_a[0:CB, cols] = moved[0:CB]
        return 0

    lax.fori_loop(0, D // wide, turn_out, 0)
    ra = [
        start(send_r.at[pl.ds(d * CB, CB)], ret_a.at[pl.ds(d * CB, CB)], ra_sem, d, plane_back[d])
        for d in range(1, G)
    ]
    slot_j = lax.broadcasted_iota(jnp.int32, (T, R), 1)
    mix = jnp.where(slot_j == slots[0], route_weights[:, 0:1], 0.0)
    mix = mix + jnp.where(slot_j == slots[1], route_weights[:, 1:2], 0.0)
    mix_hi = mix.astype(BF16)
    mix_lo = (mix - mix_hi.astype(F32)).astype(BF16)
    for copy in ra:
        copy.wait_recv()

    def combine(i, _):
        cols = pl.ds(pl.multiple_of(i * wide, wide), wide)
        rows = ret_a[0:R, cols]
        total = jnp.dot(mix_hi, rows, preferred_element_type=F32)
        total = total + jnp.dot(mix_lo, rows, preferred_element_type=F32)
        moe_out[:, cols] = total.astype(BF16)
        return 0

    lax.fori_loop(0, D // wide, combine, 0)
    for copy in pending:
        copy.wait_send()


def permutation(p):
    matrix = np.zeros((p.R, p.R), np.float32)
    for j in range(p.NZ):
        for d in range(p.G):
            for r in range(CAP):
                matrix[j * p.CB + d * CAP + r, d * p.CB + j * CAP + r] = 1.0
    return jnp.asarray(matrix, BF16)


def on_device(
    c_gate, b_gate, values, conv_taps, w_mix_out, moe_in, norm_gain,
    route_ids, route_weights, w_gate, w_up, w_down,
):
    n_ep, n_tp = lax.axis_size("ep"), lax.axis_size("tp")
    p = Plan(n_ep, n_tp, moe_in.shape[1], w_gate.shape[2], moe_in.shape[0], *c_gate.shape)
    D, F, T, R, CB, G, NZ, X = p.D, p.F, p.T, p.R, p.CB, p.G, p.NZ, p.X
    m_rows = p.TA // X
    vmem = pl.BlockSpec(memory_space=pltpu.VMEM)
    hbm = pl.BlockSpec(memory_space=pl.ANY)
    block = pltpu.VMEM((R + PAD, D), BF16)
    dma = pltpu.SemaphoreType.DMA
    return pl.pallas_call(
        functools.partial(body, p),
        name="mixer_and_experts",
        out_shape=(
            jax.ShapeDtypeStruct((m_rows, D), BF16),
            jax.ShapeDtypeStruct((T, D), BF16),
        ),
        in_specs=[vmem, vmem, vmem, vmem, hbm, vmem, vmem, vmem, vmem, vmem, hbm, hbm, hbm],
        out_specs=(vmem, vmem),
        scratch_shapes=[
            pltpu.VMEM(w_mix_out.shape, BF16),
            pltpu.VMEM((D, F), BF16),
            pltpu.VMEM((D, F), BF16),
            pltpu.VMEM((F, D), BF16),
            pltpu.VMEM((p.TA + 8, p.C), F32),
            pltpu.VMEM((8, p.C), F32),
            pltpu.VMEM((p.TA, p.C), BF16),
            pltpu.VMEM((p.TA, D), BF16),
            pltpu.VMEM((m_rows, D), BF16),
            pltpu.VMEM((m_rows, D), BF16),
            pltpu.VMEM((m_rows, D), BF16),
            pltpu.VMEM((T, D), BF16),
            block,
            block,
            block,
            pltpu.VMEM((X * R + PAD, D), BF16),
            pltpu.VMEM((X * p.GS * CB, F), BF16),
            pltpu.VMEM((X * R + PAD, D), BF16),
            block,
            block,
            block,
            block,
            block,
            block,
            block,
            dma((4,)),
            dma((2, 1)),
            dma((2, G)),
            dma((2, NZ)),
            dma((2, 2 * NZ)),
            dma((2, 2 * NZ)),
            dma((2, 6 * p.NG)),
            dma((2, 6)),
            dma((2, NZ)),
            dma((2, G)),
        ],
        compiler_params=pltpu.CompilerParams(
            collective_id=0, has_side_effects=True, vmem_limit_bytes=60 * 2**20
        ),
    )(
        c_gate, b_gate, values, conv_taps, w_mix_out, moe_in, norm_gain.reshape(1, -1),
        route_ids, route_weights, permutation(p), w_gate, w_up, w_down,
    )


def solution(mesh):
    return jax.shard_map(
        on_device,
        mesh=mesh,
        in_specs=(
            P("ep", "tp"),
            P("ep", "tp"),
            P("ep", "tp"),
            P(None, "tp"),
            P("tp", None),
            P(("ep", "tp"), None),
            P(),
            P(("ep", "tp"), None),
            P(("ep", "tp"), None),
            P("ep", None, "tp"),
            P("ep", None, "tp"),
            P("ep", "tp", None),
        ),
        out_specs=(P(("ep", "tp"), None), P(("ep", "tp"), None)),
        check_vma=False,
    )
```

time: 334 us -> 155 us (0.46)
  waiting for transfers between devices: 172 us -> 0 us
  Pallas kernels: 0 us -> 148 us
  blocking collectives: 63.2 us -> 0 us
  matrix products: 29 us -> 0 us
  starting transfers between devices: 21.6 us -> 0 us
  local copies, waits for them, and re-layouts: 21.1 us -> 6.38 us
  between operations: 14.2 us -> 0.64 us
  other arithmetic: 12.4 us -> 0 us
    pallas_call x0 -> x1, Pallas kernels: none -> 148 us  [on_device(): pl.pallas_call(functools.partial(body, p), name='mixer_and_experts', out_...]
    all_to_all x3 -> x0, waiting for transfers between devices: 113 us -> none  [the longest x2 62.6 us: sent_and_summed(): lax.all_to_all(blocks, axis, split_axis=0, concat_axis=0, tiled=True)]
    all_to_all x1 -> x0, blocking collectives: 63.2 us -> none  [on_device(): lax.all_to_all(outgoing, 'ep', split_axis=0, concat_axis=1, tiled=True)]
    all_gather x1 -> x0, waiting for transfers between devices: 55.8 us -> none  [on_device(): piece = lax.all_gather(arrived, 'tp', axis=0, tiled=True)]
    dot_general x3 -> x0, matrix products: 29 us -> none  [the longest x1 17.5 us: on_device(): jnp.dot(piece, w_down[0], preferred_element_type=jnp.float32)]
    all_to_all x3 -> x0, starting transfers between devices: 19.7 us -> none  [the longest x1 10.7 us: on_device(): lax.all_to_all(expert_out.reshape(n_ep, capacity, width), 'ep', split_axi...]
    reshape x4 -> x0, local copies, waits for them, and re-layouts: 10.2 us -> none  [the longest x1 3.66 us: on_device(): lax.all_to_all(outgoing, 'ep', split_axis=0, concat_axis=1, tiled=True)]
    reduce_sum x5 -> x0, other arithmetic: 9.8 us -> none  [the longest x2 4.54 us: sent_and_summed(): return arrived.astype(jnp.float32).sum(axis=0)]
  transfers between devices with their start and end apart: 5 -> 0, of which waited for: 5 -> 0; matrix products, arithmetic and copies ran while one was open for 2% -> 0% of each run, Pallas kernels for 0% -> 0%
where the time goes in v1:
time: 155 us
  Pallas kernels  148 us (95%)
  local copies, waits for them, and re-layouts  6.38 us (4%)
    pallas_call x1, Pallas kernels, on_device(): pl.pallas_call(functools.partial(body, p), name='mixer_and_experts', out_...  148 us
    unnamed x4, local copies, waits for them, and re-layouts  6.38 us

profile of v1, /device:TPU:8, one launch (start us, length us, event | category | flops | bytes accessed | tf_op | source)
XLA Modules:
  0.0 154.5 jit_solution(6937451498745461035)
XLA Ops:
  0.6 1.4 copy.15.route_ids
  2.0 1.4 copy.16.route_weights
  3.5 147.5 %mixer_and_experts.1 = (bf16[64,2048]{1,0:T(8,128)(2,1)}, bf16[128,2048]{1,0:T(8,128)(2,1)}) custom-call(bf16[256,256]{1,0:T(8,128)(2,1)} %c_gate.1, bf16[256,256]{1,0:T(8,128)(2,1)} %b_gate.1, bf16[256,256]{1,0:T(8,128)(2,1)} %values.1, f32[3,256]{1,0:T(4,128)} %conv_taps.1, bf16[256,2048]{1,0:T(8,128)(2,1)} %w_mix_hbm.1, bf16[128,2048]{1,0:T(8,128)(2,1)} %moe_in.1, ...), custom_call_target="tpu_custom_call" | custom-call | tf_op jit(solution)/shard_map/mixer_and_experts/pallas_call | solution.py:411
  151.0 1.7 %copy.19 = bf16[64,2048]{1,0:T(8,128)(2,1)} copy(bf16[64,2048]{1,0:T(8,128)(2,1)} %get-tuple-element.4) | data formatting | bytes 524288
  152.6 1.9 %copy.20 = bf16[128,2048]{1,0:T(8,128)(2,1)} copy(bf16[128,2048]{1,0:T(8,128)(2,1)} %get-tuple-element.5) | data formatting | bytes 1048576

commit v2 on v1

v2 whole, which is shorter than its diff:
```python
import functools
import itertools

import jax
import jax.numpy as jnp
import numpy as np
from jax import lax
from jax.experimental import pallas as pl
from jax.experimental.pallas import tpu as pltpu
from jax.sharding import PartitionSpec as P

EPS = 1e-06
MESH = pl.DeviceIdType.MESH
F32 = jnp.float32
BF16 = jnp.bfloat16
CAP = 5
PAD = 8


class Plan:
    def __init__(self, n_ep, n_tp, width, hidden, rows, tokens, channels):
        self.G = int(round(n_ep**0.5))
        self.NZ = n_ep // self.G
        assert self.G * self.NZ == n_ep and self.G == self.NZ and n_tp == 4
        self.X = n_tp
        self.D, self.F, self.T = width, hidden, rows
        self.TA, self.C = tokens, channels
        self.CB = CAP * self.G
        self.R = self.CB * self.NZ
        self.GS = 2
        self.NG = self.NZ // self.GS
        far = self.NZ // 2
        self.dz = [0]
        for step in range(1, far - 1):
            self.dz += [-step, step]
        self.dz += [far, 1 - far, far - 1]
        assert len(self.dz) == self.NZ
        self.by_distance = sorted(range(self.NZ), key=lambda j: abs(self.dz[j]))
        eighth = width // 8
        self.QA = spans([3 * eighth, 5 * eighth])
        self.QR = spans([3 * eighth, 2 * eighth, 2 * eighth, eighth])

    def off(self, k, rel, jj=0):
        return ((k * self.X + rel) * self.GS + jj) * self.CB


def spans(widths):
    ends = list(itertools.accumulate(widths))
    return [(end - width, end) for width, end in zip(widths, ends)]


def scoped(name, f, *a):
    with jax.named_scope(name):
        return f(*a)


def body(
    p,
    c_gate,
    b_gate,
    values,
    conv_taps,
    w_mix_hbm,
    moe_in,
    norm_gain,
    route_ids,
    route_weights,
    perm,
    w_gate_hbm,
    w_up_hbm,
    w_down_hbm,
    mixer_out,
    moe_out,
    w_mix,
    w_gate,
    w_up,
    w_down,
    product,
    halo,
    mixed,
    m_part,
    m_turn,
    m_minus,
    m_plus,
    normed,
    send_a,
    recv_a,
    send_b,
    gathered,
    hid,
    part,
    turn,
    s_minus,
    s_plus,
    out_b,
    ret_b,
    send_r,
    ret_a,
    mix_hi,
    mix_lo,
    w_sem,
    send_sem,
    halo_sem,
    a_sem,
    b_sem,
    ag_sem,
    fw_sem,
    rs_sem,
    mx_sem,
    rb_sem,
    ra_sem,
):
    G, NZ, X, D, F, T, CB, R, GS, NG = p.G, p.NZ, p.X, p.D, p.F, p.T, p.CB, p.R, p.GS, p.NG
    ep, x = lax.axis_index("ep"), lax.axis_index("tp")
    z, g = ep // G, ep % G

    def at(zz, gg, xx):
        return {"ep": zz * G + gg, "tp": xx}

    right, left = at(z, g, (x + 1) % X), at(z, g, (x + X - 1) % X)
    after = {"ep": (ep + 1) % (G * NZ), "tp": x}
    before = {"ep": (ep + G * NZ - 1) % (G * NZ), "tp": x}
    plane = [at(z, (g + d) % G, x) for d in range(G)]
    plane_back = [at(z, (g + G - d) % G, x) for d in range(G)]
    line = [at((z + NZ + dz) % NZ, g, x) for dz in p.dz]
    line_back = [at((z + NZ - dz) % NZ, g, x) for dz in p.dz]

    barrier = pltpu.get_barrier_semaphore()
    peers = plane[1:] + line[1:] + [right, left, after, before]
    for peer in peers:
        pl.semaphore_signal(barrier, inc=1, device_id=peer, device_id_type=MESH)

    def load(src, dst, i):
        copy = pltpu.make_async_copy(src, dst, w_sem.at[i])
        copy.start()
        return copy

    loads = [
        load(w_mix_hbm, w_mix, 0),
        load(w_gate_hbm.at[0], w_gate, 1),
        load(w_up_hbm.at[0], w_up, 2),
        load(w_down_hbm.at[0], w_down, 3),
    ]
    def start(src, dst, send, recv, peer):
        copy = pltpu.make_async_remote_copy(
            src_ref=src,
            dst_ref=dst,
            send_sem=send_sem.at[send],
            recv_sem=recv,
            device_id=peer,
            device_id_type=MESH,
        )
        copy.start()
        return copy

    def arrived(ref, recv):
        pltpu.make_async_remote_copy(
            src_ref=ref, dst_ref=ref, send_sem=send_sem.at[0], recv_sem=recv,
            device_id=right, device_id_type=MESH,
        ).wait_recv()

    def sent(ref, send):
        pltpu.make_async_remote_copy(
            src_ref=ref, dst_ref=ref, send_sem=send_sem.at[send], recv_sem=halo_sem.at[0],
            device_id=right, device_id_type=MESH,
        ).wait_send()

    HALO, A, B, AG, FW, RS, MX, RB, RA = range(9)

    tokens = p.TA
    product[8 : 8 + tokens, :] = c_gate[...].astype(F32) * values[...].astype(F32)

    stream = moe_in[...].astype(F32)
    scale = lax.rsqrt(jnp.mean(stream * stream, axis=1, keepdims=True) + EPS)
    normed[...] = (stream * scale * norm_gain[...]).astype(BF16)

    rows_i = lax.broadcasted_iota(jnp.int32, (T, T), 0)
    cols_i = lax.broadcasted_iota(jnp.int32, (T, T), 1)
    eye, earlier = rows_i == cols_i, cols_i < rows_i

    def as_row(col):
        return jnp.sum(jnp.where(eye, col, 0.0), axis=0, keepdims=True)

    def as_col(row):
        return jnp.sum(jnp.where(eye, row, 0.0), axis=1, keepdims=True)

    id_rows = [route_ids[k : k + 1, :].astype(F32) for k in range(2)]
    slots = []
    for col in [as_col(row) for row in id_rows]:
        seen = jnp.zeros((T, 1), F32)
        for row in id_rows:
            seen = seen + jnp.sum(
                jnp.where(earlier & (col == row), 1.0, 0.0), axis=1, keepdims=True
            )
        rank, expert = seen.astype(jnp.int32), col.astype(jnp.int32)
        to_g = (expert & (G - 1)) - g
        to_g = jnp.where(to_g < 0, to_g + G, to_g)
        to_z = (expert >> (G.bit_length() - 1)) - z
        to_z = jnp.where(to_z < 0, to_z + NZ, to_z)
        slot_z = jnp.zeros_like(to_z)
        for j, dz in enumerate(p.dz):
            slot_z = jnp.where(to_z == dz % NZ, j, slot_z)
        slots.append(to_g * CB + slot_z * CAP + rank)
    slot_rows = [as_row(col.astype(F32)).astype(jnp.int32) for col in slots]
    slot_i = lax.broadcasted_iota(jnp.int32, (R, T), 0)
    pick = jnp.where((slot_i == slot_rows[0]) | (slot_i == slot_rows[1]), 1.0, 0.0).astype(BF16)
    wide = min(512, D)

    def pack(i, _):
        cols = pl.ds(pl.multiple_of(i * wide, wide), wide)
        packed = jnp.dot(pick, normed[:, cols], preferred_element_type=F32).astype(BF16)
        send_a[0:R, cols] = packed
        recv_a[0:CB, cols] = packed[0:CB]
        return 0

    scoped("pack", lambda: lax.fori_loop(0, D // wide, pack, 0))
    scoped("barrier", pl.semaphore_wait, barrier, len(peers))

    start(product.at[pl.ds(tokens, 8)], halo, HALO, halo_sem.at[0], after)

    def cols_of(span):
        return pl.ds(span[0], span[1] - span[0])

    for q, span in enumerate(p.QA):
        for d in range(1, G):
            start(
                send_a.at[pl.ds(d * CB, CB), cols_of(span)],
                recv_a.at[pl.ds(d * CB, CB), cols_of(span)],
                A, a_sem.at[q], plane[d],
            )

    def rs_start(src, rows, offs, dst_off, turn, minus, plus, span, send, sems, i):
        c0, c1 = span
        mid = (c0 + c1) // 2
        lo, hi = pl.ds(c0, mid - c0), pl.ds(mid, c1 - mid)
        cols = cols_of(span)
        o0, o1, o2, o3 = (pl.ds(o, rows) for o in offs)
        od = pl.ds(dst_off, rows)
        turn_lo, turn_hi, from_minus, from_plus = (sems.at[i + n] for n in range(4))
        start(src.at[o2, lo], turn.at[od, lo], send, turn_lo, right)
        start(src.at[o2, hi], turn.at[od, hi], send, turn_hi, left)
        start(src.at[o1, hi], minus.at[od, hi], send, from_minus, right)
        start(src.at[o3, lo], plus.at[od, lo], send, from_plus, left)

        def middle():
            arrived(turn.at[od, lo], turn_lo)
            src[o1, lo] = (src[o1, lo].astype(F32) + turn[od, lo].astype(F32)).astype(BF16)
            start(src.at[o1, lo], minus.at[od, lo], send, from_minus, right)
            arrived(turn.at[od, hi], turn_hi)
            src[o3, hi] = (src[o3, hi].astype(F32) + turn[od, hi].astype(F32)).astype(BF16)
            start(src.at[o3, hi], plus.at[od, hi], send, from_plus, left)

        def end():
            arrived(minus.at[od, cols], from_minus)
            arrived(plus.at[od, cols], from_plus)
            total = src[o0, cols].astype(F32) + minus[od, cols].astype(F32)
            return (total + plus[od, cols].astype(F32)).astype(BF16)

        return middle, end

    scoped("halo", arrived, halo, halo_sem.at[0])
    product[0:8, :] = jnp.where(ep == 0, 0.0, halo[...])
    convolved = jnp.zeros((tokens, p.C), F32)
    taps = conv_taps.shape[0]
    for k in range(taps):
        convolved = convolved + conv_taps[k : k + 1, :] * product[pl.ds(8 - taps + 1 + k, tokens), :]
    mixed[...] = (b_gate[...].astype(F32) * convolved).astype(BF16)
    scoped("wmix", loads[0].wait)
    m_rows = tokens // X
    for rel in range(X):
        own = pl.ds(pl.multiple_of(((x + rel) % X) * m_rows, m_rows), m_rows)
        m_part[pl.ds(rel * m_rows, m_rows), :] = jnp.dot(
            mixed[own, :], w_mix[...], preferred_element_type=F32
        ).astype(BF16)
    m_middle, m_end = rs_start(
        m_part, m_rows, [rel * m_rows for rel in range(X)], 0, m_turn, m_minus, m_plus, (0, D), MX, mx_sem, 0
    )

    scoped("m_mid", m_middle)

    def where(j, rel):
        return pl.ds(p.off(j // GS, rel, j % GS), CB)

    def turn_in(q):
        c0, c1 = p.QA[q]
        cols = cols_of(p.QA[q])
        with jax.named_scope(f"a_wait#{q}"):
            arrived(recv_a.at[pl.ds(CB, R - CB), cols], a_sem.at[q])
        step = min(256, D // 8)

        def tile(i, _):
            part_cols = pl.ds(pl.multiple_of(c0 + i * step, step), step)
            moved = jnp.dot(perm[...], recv_a[0:R, part_cols], preferred_element_type=F32)
            moved = moved.astype(BF16)
            send_b[0:R, part_cols] = moved
            gathered[0:CB, part_cols] = moved[0:CB]
            return 0

        scoped(f"turn_in#{q}", lambda: lax.fori_loop(0, (c1 - c0) // step, tile, 0))
        for j in p.by_distance[1:] if q == 0 else p.by_distance[:0:-1]:
            start(
                send_b.at[pl.ds(j * CB, CB), cols], gathered.at[where(j, 0), cols],
                B, b_sem.at[q * NZ + j], line[j],
            )

    def gather_out(q, j):
        cols = cols_of(p.QA[q])
        i = 2 * (q * NZ + j)
        own = gathered.at[where(j, 0), cols]
        if j:
            arrived(own, b_sem.at[q * NZ + j])
        start(own, gathered.at[where(j, 3), cols], AG, ag_sem.at[i], right)
        start(own, gathered.at[where(j, 1), cols], AG, ag_sem.at[i + 1], left)

    def gather_on(q, j):
        c0, c1 = p.QA[q]
        mid = (c0 + c1) // 2
        cols, lo, hi = cols_of(p.QA[q]), pl.ds(c0, mid - c0), pl.ds(mid, c1 - mid)
        i = 2 * (q * NZ + j)
        k = j // GS
        arrived(gathered.at[where(j, 3), cols], ag_sem.at[i])
        start(gathered.at[where(j, 3), lo], gathered.at[where(j, 2), lo], FW, fw_sem.at[k], right)
        arrived(gathered.at[where(j, 1), cols], ag_sem.at[i + 1])
        start(gathered.at[where(j, 1), hi], gathered.at[where(j, 2), hi], FW, fw_sem.at[k], left)

    rows_k = X * GS * CB

    def pieces(k):
        r0 = p.off(k, 0)

        def up(t, _):
            cols = pl.ds(pl.multiple_of(t * 128, 128), 128)
            pair = jnp.concatenate([w_gate[:, cols], w_up[:, cols]], axis=1)
            both = jnp.dot(gathered[r0 : r0 + rows_k, :], pair, preferred_element_type=F32)
            hid[:, cols] = (jax.nn.silu(both[:, :128]) * both[:, 128:]).astype(BF16)
            return 0

        def down(n, _):
            cols = pl.ds(pl.multiple_of(n * wide, wide), wide)
            out = jnp.dot(hid[...], w_down[:, cols], preferred_element_type=F32).astype(BF16)
            for rel in range(X):
                to = rel * R + k * GS * CB
                part[to : to + GS * CB, cols] = out[rel * GS * CB : (rel + 1) * GS * CB]
            return 0

        def first():
            with jax.named_scope(f"cwait#{k}"):
                arrived(gathered.at[pl.ds(p.off(k, 2), GS * CB), :], fw_sem.at[k])
                if k == NG - 1:
                    for copy in loads[1:]:
                        copy.wait()
            loop(up, 0, cuts[1])

        def loop(f, lo, hi):
            with jax.named_scope(f"{f.__name__}#{k},{lo}"):
                lax.fori_loop(lo, hi, f, 0)

        tiles, outs = F // 128, D // wide
        cuts = [0, (tiles + 2) // 3, (2 * tiles + 2) // 3, tiles]
        yield first
        yield lambda: loop(up, cuts[1], cuts[2])
        yield lambda: loop(up, cuts[2], cuts[3])
        yield lambda: loop(down, 0, (outs + 1) // 2)
        yield lambda: loop(down, (outs + 1) // 2, outs)

    rs = {}
    rows_h = R // 2

    def sum_start(n):
        h, q = units[n]
        rs[n] = rs_start(
            part, rows_h, [rel * R + h * rows_h for rel in range(X)], h * rows_h,
            turn, s_minus, s_plus, p.QR[q], RS, rs_sem, 4 * n,
        )

    def sum_end(n):
        h, q = units[n]
        total = rs[n][1]()
        cols = cols_of(p.QR[q])
        out_b[h * rows_h : (h + 1) * rows_h, cols] = total
        if h == 0:
            ret_b[0:CB, cols] = total[0:CB]
        first_j = h * NZ // 2
        for j in reversed(range(max(first_j, 1), first_j + NZ // 2)):
            rows = pl.ds(j * CB, CB)
            start(out_b.at[rows, cols], ret_b.at[rows, cols], RB, rb_sem.at[q], line_back[j])

    slot_j = lax.broadcasted_iota(jnp.int32, (T, R), 1)
    w_cols = [as_col(route_weights[k : k + 1, :]) for k in range(2)]
    mix = jnp.where(slot_j == slots[0], w_cols[0], 0.0)
    mix = mix + jnp.where(slot_j == slots[1], w_cols[1], 0.0)
    mix_hi[...] = mix.astype(BF16)
    mix_lo[...] = (mix - mix_hi[...].astype(F32)).astype(BF16)

    def turn_out(q):
        cols = cols_of(p.QR[q])
        with jax.named_scope(f"rb_wait#{q}"):
            arrived(ret_b.at[pl.ds(CB, R - CB), cols], rb_sem.at[q])
        with jax.named_scope(f"turn_out#{q}"):
            moved = jnp.dot(perm[...], ret_b[0:R, cols], preferred_element_type=F32).astype(BF16)
            send_r[0:R, cols] = moved
            ret_a[0:CB, cols] = moved[0:CB]
        for d in range(1, G):
            rows = pl.ds(d * CB, CB)
            start(send_r.at[rows, cols], ret_a.at[rows, cols], RA, ra_sem.at[q], plane_back[d])

    def combine(q):
        cols = cols_of(p.QR[q])
        with jax.named_scope(f"ra_wait#{q}"):
            arrived(ret_a.at[pl.ds(CB, R - CB), cols], ra_sem.at[q])
        with jax.named_scope(f"combine#{q}"):
            rows = ret_a[0:R, cols]
            total = jnp.dot(mix_hi[...], rows, preferred_element_type=F32)
            total = total + jnp.dot(mix_lo[...], rows, preferred_element_type=F32)
            moe_out[:, cols] = total.astype(BF16)

    near_first, lead = p.by_distance, NZ // 2
    steps = [(0, j) for j in near_first[:lead]] + [(0, near_first[lead]), (1, 0)]
    steps += [(0, j) for j in near_first[lead + 1 :]] + [(1, j) for j in range(NZ - 1, 0, -1)]
    work, computed, due = [], set(), []
    on = 0

    def do_work(count):
        while count and work:
            k, piece = work.pop(0)
            piece()
            count -= 1
            if k is not None:
                computed.add(k)

    def take(k):
        for n, piece in enumerate(pieces(k)):
            work.append((k if n == 4 else None, piece))

    def step_on():
        nonlocal on
        q, j = steps[on]
        scoped(f"gon#{q},{j}", gather_on, q, j)
        on += 1
        while due:
            take(due.pop(0))
        if q == 1 and j and (j % GS == 0 or j == 1):
            due.append(j // GS)

    turn_in(0)
    for n, (q, j) in enumerate(steps):
        if n == lead:
            turn_in(1)
        scoped(f"gout#{q},{j}", gather_out, q, j)
        ahead = 1 if n <= NZ else 2
        while on + ahead <= n:
            step_on()
            do_work(2)
    with jax.named_scope("m_end"):
        mixer_out[...] = m_end()
    while on < len(steps):
        step_on()
        do_work(2)
    while due:
        take(due.pop(0))
    last = len(p.QR) - 1
    far_units, near_units = [(1, q) for q in range(last + 1)], [(0, q) for q in range(last + 1)]
    units = far_units[:last] + near_units[:1] + far_units[last:] + near_units[1:]
    begun = 0
    for n in range(len(units) + 1):
        while begun < len(units) and begun <= n + 2:
            half_groups = range(NG // 2, NG) if units[begun][0] else range(NG // 2)
            if not computed.issuperset(half_groups):
                if begun > n and units[begun][0] == 0:
                    break
                while not computed.issuperset(half_groups):
                    do_work(1)
            scoped(f"sstart#{begun}", sum_start, begun)
            begun += 1
        if n < len(units):
            do_work(2)
            scoped(f"smid#{n}", rs[n][0])
        if n >= 1:
            scoped(f"send#{n - 1}", sum_end, n - 1)
            h, q = units[n - 1]
            if h == 0 and q:
                turn_out(q - 1)
                if q >= 2:
                    combine(q - 2)
    turn_out(last)
    combine(last - 1)
    combine(last)
    with jax.named_scope("sends"):
        sent(halo, HALO)
        sent(send_a.at[pl.ds(CB, R - CB), :], A)
        sent(send_b.at[pl.ds(CB, R - CB), :], B)
        sent(gathered.at[pl.ds(0, 2 * R), :], AG)
        sent(gathered.at[pl.ds(0, R), :], FW)
        sent(part.at[pl.ds(0, 3 * R), :], RS)
        sent(m_part.at[pl.ds(0, 3 * m_rows), :], MX)
        sent(out_b.at[pl.ds(CB, R - CB), :], RB)
        sent(send_r.at[pl.ds(CB, R - CB), :], RA)


def permutation(p):
    matrix = np.zeros((p.R, p.R), np.float32)
    for j in range(p.NZ):
        for d in range(p.G):
            for r in range(CAP):
                matrix[j * p.CB + d * CAP + r, d * p.CB + j * CAP + r] = 1.0
    return jnp.asarray(matrix, BF16)


def on_device(
    c_gate, b_gate, values, conv_taps, w_mix_out, moe_in, norm_gain,
    route_ids, route_weights, w_gate, w_up, w_down,
):
    n_ep, n_tp = lax.axis_size("ep"), lax.axis_size("tp")
    p = Plan(n_ep, n_tp, moe_in.shape[1], w_gate.shape[2], moe_in.shape[0], *c_gate.shape)
    D, F, T, R, CB, G, NZ, X = p.D, p.F, p.T, p.R, p.CB, p.G, p.NZ, p.X
    m_rows = p.TA // X
    vmem = pl.BlockSpec(memory_space=pltpu.VMEM)
    hbm = pl.BlockSpec(memory_space=pl.ANY)
    block = pltpu.VMEM((R + PAD, D), BF16)
    dma = pltpu.SemaphoreType.DMA
    return pl.pallas_call(
        functools.partial(body, p),
        name="mixer_and_experts",
        out_shape=(
            jax.ShapeDtypeStruct((m_rows, D), BF16),
            jax.ShapeDtypeStruct((T, D), BF16),
        ),
        in_specs=[vmem, vmem, vmem, vmem, hbm, vmem, vmem, vmem, vmem, vmem, hbm, hbm, hbm],
        out_specs=(vmem, vmem),
        scratch_shapes=[
            pltpu.VMEM(w_mix_out.shape, BF16),
            pltpu.VMEM((D, F), BF16),
            pltpu.VMEM((D, F), BF16),
            pltpu.VMEM((F, D), BF16),
            pltpu.VMEM((p.TA + 8, p.C), F32),
            pltpu.VMEM((8, p.C), F32),
            pltpu.VMEM((p.TA, p.C), BF16),
            pltpu.VMEM((p.TA, D), BF16),
            pltpu.VMEM((m_rows, D), BF16),
            pltpu.VMEM((m_rows, D), BF16),
            pltpu.VMEM((m_rows, D), BF16),
            pltpu.VMEM((T, D), BF16),
            block,
            block,
            block,
            pltpu.VMEM((X * R + PAD, D), BF16),
            pltpu.VMEM((X * p.GS * CB, F), BF16),
            pltpu.VMEM((X * R + PAD, D), BF16),
            block,
            block,
            block,
            block,
            block,
            block,
            block,
            pltpu.VMEM((T, R), BF16),
            pltpu.VMEM((T, R), BF16),
            dma((4,)),
            dma((9,)),
            dma((1,)),
            dma((len(p.QA),)),
            dma((len(p.QA) * NZ,)),
            dma((len(p.QA) * 2 * NZ,)),
            dma((p.NG,)),
            dma((4 * 2 * len(p.QR),)),
            dma((4,)),
            dma((len(p.QR),)),
            dma((len(p.QR),)),
        ],
        compiler_params=pltpu.CompilerParams(
            collective_id=0, has_side_effects=True, vmem_limit_bytes=60 * 2**20
        ),
    )(
        c_gate, b_gate, values, conv_taps, w_mix_out, moe_in, norm_gain.reshape(1, -1),
        route_ids.T, route_weights.T, permutation(p), w_gate, w_up, w_down,
    )


def solution(mesh):
    return jax.shard_map(
        on_device,
        mesh=mesh,
        in_specs=(
            P("ep", "tp"),
            P("ep", "tp"),
            P("ep", "tp"),
            P(None, "tp"),
            P("tp", None),
            P(("ep", "tp"), None),
            P(),
            P(("ep", "tp"), None),
            P(("ep", "tp"), None),
            P("ep", None, "tp"),
            P("ep", None, "tp"),
            P("ep", "tp", None),
        ),
        out_specs=(P(("ep", "tp"), None), P(("ep", "tp"), None)),
        check_vma=False,
    )
```

time: 155 us -> 145 us (0.935)
  Pallas kernels: 148 us -> 139 us
  local copies, waits for them, and re-layouts: 6.38 us -> 3.55 us
    pallas_call x1, Pallas kernels: 148 us -> 139 us  [on_device(): pl.pallas_call(functools.partial(body, p), name='mixer_and_experts', out_...]
    unnamed x4 -> x2, local copies, waits for them, and re-layouts: 6.38 us -> 3.55 us
where the time goes in v2:
time: 145 us; the launch traced here: 144 us
  Pallas kernels  139 us (96%)
  local copies, waits for them, and re-layouts  3.55 us (2%)
    pallas_call x1, Pallas kernels, on_device(): pl.pallas_call(functools.partial(body, p), name='mixer_and_experts', out_...  139 us
    unnamed x2, local copies, waits for them, and re-layouts  3.55 us

profile of v2, /device:TPU:8, one launch (start us, length us, event | category | flops | bytes accessed | tf_op | source)
XLA Modules:
  0.0 143.5 jit_solution(7969868475953316906)
XLA Ops:
  0.6 139.3 %mixer_and_experts.1 = (bf16[64,2048]{1,0:T(8,128)(2,1)}, bf16[128,2048]{1,0:T(8,128)(2,1)}) custom-call(bf16[256,256]{1,0:T(8,128)(2,1)} %c_gate.1, bf16[256,256]{1,0:T(8,128)(2,1)} %b_gate.1, bf16[256,256]{1,0:T(8,128)(2,1)} %values.1, f32[3,256]{1,0:T(4,128)} %conv_taps.1, bf16[256,2048]{1,0:T(8,128)(2,1)} %w_mix_hbm.1, bf16[128,2048]{1,0:T(8,128)(2,1)} %moe_in.1, ...), custom_call_target="tpu_custom_call" | custom-call | tf_op jit(solution)/shard_map/mixer_and_experts/pallas_call | solution.py:521
  140.0 1.7 %copy.17 = bf16[64,2048]{1,0:T(8,128)(2,1)} copy(bf16[64,2048]{1,0:T(8,128)(2,1)} %get-tuple-element.4) | data formatting | bytes 524288
  141.6 1.9 %copy.18 = bf16[128,2048]{1,0:T(8,128)(2,1)} copy(bf16[128,2048]{1,0:T(8,128)(2,1)} %get-tuple-element.5) | data formatting | bytes 1048576

commit v3 on v2

--- a/solution.py
+++ b/solution.py
@@ -35,10 +35,13 @@
             self.dz += [-step, step]
         self.dz += [far, 1 - far, far - 1]
         assert len(self.dz) == self.NZ
-        self.by_distance = sorted(range(self.NZ), key=lambda j: abs(self.dz[j]))
+        near_first = sorted(range(1, self.NZ), key=lambda j: abs(self.dz[j]))
+        self.sends = [near_first, [1, 2] + list(range(self.NZ - 1, 2, -1))]
         eighth = width // 8
-        self.QA = spans([3 * eighth, 5 * eighth])
+        self.QA = spans([2 * eighth, 6 * eighth])
         self.QR = spans([3 * eighth, 2 * eighth, 2 * eighth, eighth])
+        self.QF = spans([5 * eighth, 3 * eighth])
+        assert self.NZ == 8
 
     def off(self, k, rel, jj=0):
         return ((k * self.X + rel) * self.GS + jj) * self.CB
@@ -214,6 +217,24 @@
         return 0
 
     scoped("pack", lambda: lax.fori_loop(0, D // wide, pack, 0))
+
+    def convolve(first, count):
+        taps = conv_taps.shape[0]
+        convolved = jnp.zeros((count, p.C), F32)
+        for k in range(taps):
+            reach = product[8 - taps + 1 + k + first : 8 - taps + 1 + k + first + count, :]
+            convolved = convolved + conv_taps[k : k + 1, :] * reach
+        return (b_gate[first : first + count, :].astype(F32) * convolved).astype(BF16)
+
+    product[0:8, :] = jnp.zeros((8, p.C), F32)
+    mixed[...] = convolve(0, tokens)
+    scoped("wmix", loads[0].wait)
+    m_rows = tokens // X
+    for rel in range(X):
+        own = pl.ds(pl.multiple_of(((x + rel) % X) * m_rows, m_rows), m_rows)
+        m_part[pl.ds(rel * m_rows, m_rows), :] = jnp.dot(
+            mixed[own, :], w_mix[...], preferred_element_type=F32
+        ).astype(BF16)
     scoped("barrier", pl.semaphore_wait, barrier, len(peers))
 
     start(product.at[pl.ds(tokens, 8)], halo, HALO, halo_sem.at[0], after)
@@ -221,13 +242,13 @@
     def cols_of(span):
         return pl.ds(span[0], span[1] - span[0])
 
-    for q, span in enumerate(p.QA):
+    def send_out(q):
+        cols = cols_of(p.QA[q])
         for d in range(1, G):
-            start(
-                send_a.at[pl.ds(d * CB, CB), cols_of(span)],
-                recv_a.at[pl.ds(d * CB, CB), cols_of(span)],
-                A, a_sem.at[q], plane[d],
-            )
+            rows = pl.ds(d * CB, CB)
+            start(send_a.at[rows, cols], recv_a.at[rows, cols], A + 9 * q, a_sem.at[q], plane[d])
+
+    send_out(0)
 
     def rs_start(src, rows, offs, dst_off, turn, minus, plus, span, send, sems, i):
         c0, c1 = span
@@ -260,22 +281,19 @@
 
     scoped("halo", arrived, halo, halo_sem.at[0])
     product[0:8, :] = jnp.where(ep == 0, 0.0, halo[...])
-    convolved = jnp.zeros((tokens, p.C), F32)
-    taps = conv_taps.shape[0]
-    for k in range(taps):
-        convolved = convolved + conv_taps[k : k + 1, :] * product[pl.ds(8 - taps + 1 + k, tokens), :]
-    mixed[...] = (b_gate[...].astype(F32) * convolved).astype(BF16)
-    scoped("wmix", loads[0].wait)
-    m_rows = tokens // X
-    for rel in range(X):
-        own = pl.ds(pl.multiple_of(((x + rel) % X) * m_rows, m_rows), m_rows)
-        m_part[pl.ds(rel * m_rows, m_rows), :] = jnp.dot(
-            mixed[own, :], w_mix[...], preferred_element_type=F32
-        ).astype(BF16)
+    top = 16
+    mixed[0:top, :] = convolve(0, top)
+    to_top = pl.multiple_of(((X - x) % X) * m_rows, m_rows)
+    m_part[pl.ds(to_top, top), :] = jnp.dot(
+        mixed[0:top, :], w_mix[...], preferred_element_type=F32
+    ).astype(BF16)
     m_middle, m_end = rs_start(
         m_part, m_rows, [rel * m_rows for rel in range(X)], 0, m_turn, m_minus, m_plus, (0, D), MX, mx_sem, 0
     )
 
+    with jax.named_scope("a_sent"):
+        sent(send_a.at[pl.ds(CB, R - CB), cols_of(p.QA[0])], A)
+    send_out(1)
     scoped("m_mid", m_middle)
 
     def where(j, rel):
@@ -297,7 +315,7 @@
             return 0
 
         scoped(f"turn_in#{q}", lambda: lax.fori_loop(0, (c1 - c0) // step, tile, 0))
-        for j in p.by_distance[1:] if q == 0 else p.by_distance[:0:-1]:
+        for j in p.sends[q]:
             start(
                 send_b.at[pl.ds(j * CB, CB), cols], gathered.at[where(j, 0), cols],
                 B, b_sem.at[q * NZ + j], line[j],
@@ -336,7 +354,7 @@
             return 0
 
         def down(n, _):
-            cols = pl.ds(pl.multiple_of(n * wide, wide), wide)
+            cols = pl.ds(pl.multiple_of(n * (D // 2), 128), D // 2)
             out = jnp.dot(hid[...], w_down[:, cols], preferred_element_type=F32).astype(BF16)
             for rel in range(X):
                 to = rel * R + k * GS * CB
@@ -346,7 +364,7 @@
         def first():
             with jax.named_scope(f"cwait#{k}"):
                 arrived(gathered.at[pl.ds(p.off(k, 2), GS * CB), :], fw_sem.at[k])
-                if k == NG - 1:
+                if k == 0:
                     for copy in loads[1:]:
                         copy.wait()
             loop(up, 0, cuts[1])
@@ -355,7 +373,7 @@
             with jax.named_scope(f"{f.__name__}#{k},{lo}"):
                 lax.fori_loop(lo, hi, f, 0)
 
-        tiles, outs = F // 128, D // wide
+        tiles, outs = F // 128, 2
         cuts = [0, (tiles + 2) // 3, (2 * tiles + 2) // 3, tiles]
         yield first
         yield lambda: loop(up, cuts[1], cuts[2])
@@ -364,27 +382,34 @@
         yield lambda: loop(down, (outs + 1) // 2, outs)
 
     rs = {}
-    rows_h = R // 2
+    half = NZ // 2
+    far_units = [(k * GS, GS, span) for span in p.QF for k in range(NG - 1, NG // 2 - 1, -1)]
+    units = far_units + [(0, half, span) for span in p.QR]
+    units = units[:2] + units[4:5] + units[2:4] + units[5:]
 
     def sum_start(n):
-        h, q = units[n]
+        j, count, span = units[n]
         rs[n] = rs_start(
-            part, rows_h, [rel * R + h * rows_h for rel in range(X)], h * rows_h,
-            turn, s_minus, s_plus, p.QR[q], RS, rs_sem, 4 * n,
+            part, count * CB, [rel * R + j * CB for rel in range(X)], j * CB,
+            turn, s_minus, s_plus, span, RS, rs_sem, 4 * n,
         )
 
+    def back_sem(n):
+        span = units[n][2]
+        return rb_sem.at[p.QF.index(span)] if units[n][0] else rb_sem.at[len(p.QF) + p.QR.index(span)]
+
     def sum_end(n):
-        h, q = units[n]
+        j0, count, span = units[n]
         total = rs[n][1]()
-        cols = cols_of(p.QR[q])
-        out_b[h * rows_h : (h + 1) * rows_h, cols] = total
-        if h == 0:
+        cols = cols_of(span)
+        out_b[j0 * CB : (j0 + count) * CB, cols] = total
+        if j0 == 0:
             ret_b[0:CB, cols] = total[0:CB]
-        first_j = h * NZ // 2
-        for j in reversed(range(max(first_j, 1), first_j + NZ // 2)):
+        for j in reversed(range(max(j0, 1), j0 + count)):
             rows = pl.ds(j * CB, CB)
-            start(out_b.at[rows, cols], ret_b.at[rows, cols], RB, rb_sem.at[q], line_back[j])
-
+            start(out_b.at[rows, cols], ret_b.at[rows, cols], RB, back_sem(n), line_back[j])
+
+    far_back = set()
     slot_j = lax.broadcasted_iota(jnp.int32, (T, R), 1)
     w_cols = [as_col(route_weights[k : k + 1, :]) for k in range(2)]
     mix = jnp.where(slot_j == slots[0], w_cols[0], 0.0)
@@ -395,7 +420,11 @@
     def turn_out(q):
         cols = cols_of(p.QR[q])
         with jax.named_scope(f"rb_wait#{q}"):
-            arrived(ret_b.at[pl.ds(CB, R - CB), cols], rb_sem.at[q])
+            for i, span in enumerate(p.QF):
+                if span[0] < p.QR[q][1] and i not in far_back:
+                    far_back.add(i)
+                    arrived(ret_b.at[pl.ds(half * CB, R - half * CB), cols_of(span)], rb_sem.at[i])
+            arrived(ret_b.at[pl.ds(CB, (half - 1) * CB), cols], rb_sem.at[len(p.QF) + q])
         with jax.named_scope(f"turn_out#{q}"):
             moved = jnp.dot(perm[...], ret_b[0:R, cols], preferred_element_type=F32).astype(BF16)
             send_r[0:R, cols] = moved
@@ -414,80 +443,60 @@
             total = total + jnp.dot(mix_lo[...], rows, preferred_element_type=F32)
             moe_out[:, cols] = total.astype(BF16)
 
-    near_first, lead = p.by_distance, NZ // 2
-    steps = [(0, j) for j in near_first[:lead]] + [(0, near_first[lead]), (1, 0)]
-    steps += [(0, j) for j in near_first[lead + 1 :]] + [(1, j) for j in range(NZ - 1, 0, -1)]
-    work, computed, due = [], set(), []
-    on = 0
+    work, computed = [], set()
 
     def do_work(count):
         while count and work:
-            k, piece = work.pop(0)
+            k, n, piece = work.pop(0)
             piece()
             count -= 1
-            if k is not None:
+            if n == 4:
                 computed.add(k)
 
-    def take(k):
-        for n, piece in enumerate(pieces(k)):
-            work.append((k if n == 4 else None, piece))
-
-    def step_on():
-        nonlocal on
-        q, j = steps[on]
-        scoped(f"gon#{q},{j}", gather_on, q, j)
-        on += 1
-        while due:
-            take(due.pop(0))
-        if q == 1 and j and (j % GS == 0 or j == 1):
-            due.append(j // GS)
-
-    turn_in(0)
-    for n, (q, j) in enumerate(steps):
-        if n == lead:
-            turn_in(1)
-        scoped(f"gout#{q},{j}", gather_out, q, j)
-        ahead = 1 if n <= NZ else 2
-        while on + ahead <= n:
-            step_on()
-            do_work(2)
-    with jax.named_scope("m_end"):
-        mixer_out[...] = m_end()
-    while on < len(steps):
-        step_on()
-        do_work(2)
-    while due:
-        take(due.pop(0))
-    last = len(p.QR) - 1
-    far_units, near_units = [(1, q) for q in range(last + 1)], [(0, q) for q in range(last + 1)]
-    units = far_units[:last] + near_units[:1] + far_units[last:] + near_units[1:]
-    begun = 0
+    script = """
+        t0 o00 o01 n00 o02 n01 o03 n02 o04 t1 n03 o10 o06 o07 n04 n06 n07 o05 n10 n05
+        o11 o12 n11 o17 o16 n12 w0 c1 n17 o15 c1 n16 c2 o14 o13 c1 n15 w3 c1 n14 c2 n13 c2
+        s0 m w2 c3 i0 c2 s1 w1 c3 i1 c2 s2
+    """
+    for event in script.split():
+        kind, at_n = event[0], [int(digit) for digit in event[1:]]
+        if kind == "t":
+            turn_in(*at_n)
+        elif kind == "o":
+            scoped("gout#" + event, gather_out, *at_n)
+        elif kind == "n":
+            scoped("gon#" + event, gather_on, *at_n)
+        elif kind == "w":
+            work.extend((at_n[0], n, piece) for n, piece in enumerate(pieces(at_n[0])))
+        elif kind == "c":
+            do_work(*at_n)
+        elif kind == "s":
+            scoped("sstart#" + event, sum_start, *at_n)
+        elif kind == "i":
+            scoped("smid#" + event, rs[at_n[0]][0])
+        elif kind == "m":
+            with jax.named_scope("m_end"):
+                mixer_out[...] = m_end()
+    last, turns = len(p.QR) - 1, {4: 0}
+    begun = 3
     for n in range(len(units) + 1):
         while begun < len(units) and begun <= n + 2:
-            half_groups = range(NG // 2, NG) if units[begun][0] else range(NG // 2)
-            if not computed.issuperset(half_groups):
-                if begun > n and units[begun][0] == 0:
-                    break
-                while not computed.issuperset(half_groups):
-                    do_work(1)
             scoped(f"sstart#{begun}", sum_start, begun)
             begun += 1
-        if n < len(units):
-            do_work(2)
+        if 2 <= n < len(units):
             scoped(f"smid#{n}", rs[n][0])
         if n >= 1:
             scoped(f"send#{n - 1}", sum_end, n - 1)
-            h, q = units[n - 1]
-            if h == 0 and q:
-                turn_out(q - 1)
-                if q >= 2:
-                    combine(q - 2)
+        if n - 1 in turns:
+            turn_out(turns[n - 1])
+    turn_out(1)
+    turn_out(2)
     turn_out(last)
-    combine(last - 1)
-    combine(last)
+    for q in range(last + 1):
+        combine(q)
     with jax.named_scope("sends"):
         sent(halo, HALO)
-        sent(send_a.at[pl.ds(CB, R - CB), :], A)
+        sent(send_a.at[pl.ds(CB, R - CB), cols_of(p.QA[1])], A + 9)
         sent(send_b.at[pl.ds(CB, R - CB), :], B)
         sent(gathered.at[pl.ds(0, 2 * R), :], AG)
         sent(gathered.at[pl.ds(0, R), :], FW)
@@ -556,15 +565,15 @@
             pltpu.VMEM((T, R), BF16),
             pltpu.VMEM((T, R), BF16),
             dma((4,)),
-            dma((9,)),
+            dma((11,)),
             dma((1,)),
             dma((len(p.QA),)),
             dma((len(p.QA) * NZ,)),
             dma((len(p.QA) * 2 * NZ,)),
             dma((p.NG,)),
-            dma((4 * 2 * len(p.QR),)),
+            dma((4 * (p.NG // 2 * len(p.QF) + len(p.QR)),)),
             dma((4,)),
-            dma((len(p.QR),)),
+            dma((len(p.QF) + len(p.QR),)),
             dma((len(p.QR),)),
         ],
         compiler_params=pltpu.CompilerParams(

time: 145 us -> 131 us (0.903)
  Pallas kernels: 139 us -> 126 us
    pallas_call x1, Pallas kernels: 139 us -> 126 us  [on_device(): pl.pallas_call(functools.partial(body, p), name='mixer_and_experts', out_...]
where the time goes in v3:
time: 131 us
  Pallas kernels  126 us (96%)
  local copies, waits for them, and re-layouts  3.55 us (3%)
    pallas_call x1, Pallas kernels, on_device(): pl.pallas_call(functools.partial(body, p), name='mixer_and_experts', out_...  126 us
    unnamed x2, local copies, waits for them, and re-layouts  3.55 us

profile of v3, /device:TPU:8, one launch (start us, length us, event | category | flops | bytes accessed | tf_op | source)
XLA Modules:
  0.0 130.6 jit_solution(8374783756649852209)
XLA Ops:
  0.6 126.4 %mixer_and_experts.1 = (bf16[64,2048]{1,0:T(8,128)(2,1)}, bf16[128,2048]{1,0:T(8,128)(2,1)}) custom-call(bf16[256,256]{1,0:T(8,128)(2,1)} %c_gate.1, bf16[256,256]{1,0:T(8,128)(2,1)} %b_gate.1, bf16[256,256]{1,0:T(8,128)(2,1)} %values.1, f32[3,256]{1,0:T(4,128)} %conv_taps.1, bf16[256,2048]{1,0:T(8,128)(2,1)} %w_mix_hbm.1, bf16[128,2048]{1,0:T(8,128)(2,1)} %moe_in.1, ...), custom_call_target="tpu_custom_call" | custom-call | tf_op jit(solution)/shard_map/mixer_and_experts/pallas_call | solution.py:530
  127.0 1.7 %copy.17 = bf16[64,2048]{1,0:T(8,128)(2,1)} copy(bf16[64,2048]{1,0:T(8,128)(2,1)} %get-tuple-element.4) | data formatting | bytes 524288
  128.7 1.9 %copy.18 = bf16[128,2048]{1,0:T(8,128)(2,1)} copy(bf16[128,2048]{1,0:T(8,128)(2,1)} %get-tuple-element.5) | data formatting | bytes 1048576

commit v4 on v3

--- a/solution.py
+++ b/solution.py
@@ -38,9 +38,9 @@
         near_first = sorted(range(1, self.NZ), key=lambda j: abs(self.dz[j]))
         self.sends = [near_first, [1, 2] + list(range(self.NZ - 1, 2, -1))]
         eighth = width // 8
-        self.QA = spans([2 * eighth, 6 * eighth])
-        self.QR = spans([3 * eighth, 2 * eighth, 2 * eighth, eighth])
-        self.QF = spans([5 * eighth, 3 * eighth])
+        self.QA = spans([3 * eighth, 5 * eighth])
+        self.QR = spans([4 * eighth, 2 * eighth, eighth, eighth])
+        self.QF = spans([6 * eighth, 2 * eighth])
         assert self.NZ == 8
 
     def off(self, k, rel, jj=0):
@@ -453,12 +453,23 @@
             if n == 4:
                 computed.add(k)
 
-    script = """
-        t0 o00 o01 n00 o02 n01 o03 n02 o04 t1 n03 o10 o06 o07 n04 n06 n07 o05 n10 n05
-        o11 o12 n11 o17 o16 n12 w0 c1 n17 o15 c1 n16 c2 o14 o13 c1 n15 w3 c1 n14 c2 n13 c2
-        s0 m w2 c3 i0 c2 s1 w1 c3 i1 c2 s2
-    """
-    for event in script.split():
+    script = (
+        "t0 o00 o01 n00",
+        "o02 n01 o03 n02",
+        "o04 t1 n03 o10",
+        "o06 o07 n04 o05",
+        "n10 o11 o12 n06",
+        "n07 n05 n11 o17",
+        "o16 n12 w0 c1",
+        "n17 o15 c1 n16",
+        "c2 o14 o13 c1",
+        "n15 w3 c1 n14",
+        "c2 n13 c2 s0",
+        "m w2 c3 i0",
+        "c2 s1 w1 c3",
+        "i1 c2 s2",
+    )
+    for event in itertools.chain(*(line.split() for line in script)):
         kind, at_n = event[0], [int(digit) for digit in event[1:]]
         if kind == "t":
             turn_in(*at_n)
@@ -506,6 +517,12 @@
         sent(send_r.at[pl.ds(CB, R - CB), :], RA)
 
 
+def hand_over(*refs):
+    count = len(refs) // 2
+    for source, target in zip(refs[:count], refs[count:]):
+        target[...] = source[...]
+
+
 def permutation(p):
     matrix = np.zeros((p.R, p.R), np.float32)
     for j in range(p.NZ):
@@ -527,7 +544,7 @@
     hbm = pl.BlockSpec(memory_space=pl.ANY)
     block = pltpu.VMEM((R + PAD, D), BF16)
     dma = pltpu.SemaphoreType.DMA
-    return pl.pallas_call(
+    outs = pl.pallas_call(
         functools.partial(body, p),
         name="mixer_and_experts",
         out_shape=(
@@ -583,6 +600,13 @@
         c_gate, b_gate, values, conv_taps, w_mix_out, moe_in, norm_gain.reshape(1, -1),
         route_ids.T, route_weights.T, permutation(p), w_gate, w_up, w_down,
     )
+    return pl.pallas_call(
+        hand_over,
+        name="hand_over",
+        out_shape=tuple(jax.ShapeDtypeStruct(out.shape, out.dtype) for out in outs),
+        in_specs=[vmem] * len(outs),
+        out_specs=tuple([vmem] * len(outs)),
+    )(*outs)
 
 
 def solution(mesh):

time: 131 us -> 128 us (0.977)
  local copies, waits for them, and re-layouts: 3.55 us -> 0 us
    unnamed x2 -> x0, local copies, waits for them, and re-layouts: 3.55 us -> none
    pallas_call x0 -> x1, Pallas kernels: none -> 2.02 us  [on_device(): pl.pallas_call(hand_over, name='hand_over', out_shape=tuple((jax.ShapeDty...]
    pallas_call x1, Pallas kernels: 126 us -> 125 us  [on_device(): pl.pallas_call(functools.partial(body, p), name='mixer_and_experts', out_...]
where the time goes in v4:
time: 128 us; the launch traced here: 127 us
  Pallas kernels  127 us (99%)
    pallas_call x1, Pallas kernels, on_device(): pl.pallas_call(functools.partial(body, p), name='mixer_and_experts', out_...  125 us

profile of v4, /device:TPU:8, one launch (start us, length us, event | category | flops | bytes accessed | tf_op | source)
XLA Modules:
  0.0 127.5 jit_solution(2189043660402662483)
XLA Ops:
  0.6 124.8 %mixer_and_experts.1 = (bf16[64,2048]{1,0:T(8,128)(2,1)}, bf16[128,2048]{1,0:T(8,128)(2,1)}) custom-call(bf16[256,256]{1,0:T(8,128)(2,1)} %c_gate.1, bf16[256,256]{1,0:T(8,128)(2,1)} %b_gate.1, bf16[256,256]{1,0:T(8,128)(2,1)} %values.1, f32[3,256]{1,0:T(4,128)} %conv_taps.1, bf16[256,2048]{1,0:T(8,128)(2,1)} %w_mix_hbm.1, bf16[128,2048]{1,0:T(8,128)(2,1)} %moe_in.1, ...), custom_call_target="tpu_custom_call" | custom-call | tf_op jit(solution)/shard_map/mixer_and_experts/pallas_call | solution.py:547
  125.5 2.0 %hand_over.1 = (bf16[64,2048]{1,0:T(8,128)(2,1)}, bf16[128,2048]{1,0:T(8,128)(2,1)}) custom-call(bf16[64,2048]{1,0:T(8,128)(2,1)} %get-tuple-element.4.refs_0_, bf16[128,2048]{1,0:T(8,128)(2,1)} %get-tuple-element.5.refs_1_), custom_call_target="tpu_custom_call" | custom-call | tf_op jit(solution)/shard_map/hand_over/pallas_call | solution.py:603

commit v5 on v4

--- a/solution.py
+++ b/solution.py
@@ -218,23 +218,6 @@
 
     scoped("pack", lambda: lax.fori_loop(0, D // wide, pack, 0))
 
-    def convolve(first, count):
-        taps = conv_taps.shape[0]
-        convolved = jnp.zeros((count, p.C), F32)
-        for k in range(taps):
-            reach = product[8 - taps + 1 + k + first : 8 - taps + 1 + k + first + count, :]
-            convolved = convolved + conv_taps[k : k + 1, :] * reach
-        return (b_gate[first : first + count, :].astype(F32) * convolved).astype(BF16)
-
-    product[0:8, :] = jnp.zeros((8, p.C), F32)
-    mixed[...] = convolve(0, tokens)
-    scoped("wmix", loads[0].wait)
-    m_rows = tokens // X
-    for rel in range(X):
-        own = pl.ds(pl.multiple_of(((x + rel) % X) * m_rows, m_rows), m_rows)
-        m_part[pl.ds(rel * m_rows, m_rows), :] = jnp.dot(
-            mixed[own, :], w_mix[...], preferred_element_type=F32
-        ).astype(BF16)
     scoped("barrier", pl.semaphore_wait, barrier, len(peers))
 
     start(product.at[pl.ds(tokens, 8)], halo, HALO, halo_sem.at[0], after)
@@ -279,6 +262,23 @@
 
         return middle, end
 
+    def convolve(first, count):
+        taps = conv_taps.shape[0]
+        convolved = jnp.zeros((count, p.C), F32)
+        for k in range(taps):
+            reach = product[8 - taps + 1 + k + first : 8 - taps + 1 + k + first + count, :]
+            convolved = convolved + conv_taps[k : k + 1, :] * reach
+        return (b_gate[first : first + count, :].astype(F32) * convolved).astype(BF16)
+
+    product[0:8, :] = jnp.zeros((8, p.C), F32)
+    mixed[...] = convolve(0, tokens)
+    scoped("wmix", loads[0].wait)
+    m_rows = tokens // X
+    for rel in range(X):
+        own = pl.ds(pl.multiple_of(((x + rel) % X) * m_rows, m_rows), m_rows)
+        m_part[pl.ds(rel * m_rows, m_rows), :] = jnp.dot(
+            mixed[own, :], w_mix[...], preferred_element_type=F32
+        ).astype(BF16)
     scoped("halo", arrived, halo, halo_sem.at[0])
     product[0:8, :] = jnp.where(ep == 0, 0.0, halo[...])
     top = 16
@@ -467,7 +467,7 @@
         "c2 n13 c2 s0",
         "m w2 c3 i0",
         "c2 s1 w1 c3",
-        "i1 c2 s2",
+        "s3 i1 c2 s2",
     )
     for event in itertools.chain(*(line.split() for line in script)):
         kind, at_n = event[0], [int(digit) for digit in event[1:]]
@@ -489,7 +489,7 @@
             with jax.named_scope("m_end"):
                 mixer_out[...] = m_end()
     last, turns = len(p.QR) - 1, {4: 0}
-    begun = 3
+    begun = 4
     for n in range(len(units) + 1):
         while begun < len(units) and begun <= n + 2:
             scoped(f"sstart#{begun}", sum_start, begun)

time: 128 us -> 128 us (level)
  no operation moved by 1% of the time
where the time goes in v5:
time: 128 us; the launch traced here: 127 us
  Pallas kernels  126 us (98%)
    pallas_call x1, Pallas kernels, on_device(): pl.pallas_call(functools.partial(body, p), name='mixer_and_experts', out_...  124 us

profile of v5, /device:TPU:8, one launch (start us, length us, event | category | flops | bytes accessed | tf_op | source)
XLA Modules:
  0.0 126.7 jit_solution(1907476944801725227)
XLA Ops:
  0.6 124.0 %mixer_and_experts.1 = (bf16[64,2048]{1,0:T(8,128)(2,1)}, bf16[128,2048]{1,0:T(8,128)(2,1)}) custom-call(bf16[256,256]{1,0:T(8,128)(2,1)} %c_gate.1, bf16[256,256]{1,0:T(8,128)(2,1)} %b_gate.1, bf16[256,256]{1,0:T(8,128)(2,1)} %values.1, f32[3,256]{1,0:T(4,128)} %conv_taps.1, bf16[256,2048]{1,0:T(8,128)(2,1)} %w_mix_hbm.1, bf16[128,2048]{1,0:T(8,128)(2,1)} %moe_in.1, ...), custom_call_target="tpu_custom_call" | custom-call | tf_op jit(solution)/shard_map/mixer_and_experts/pallas_call | solution.py:547
  124.7 2.0 %hand_over.1 = (bf16[64,2048]{1,0:T(8,128)(2,1)}, bf16[128,2048]{1,0:T(8,128)(2,1)}) custom-call(bf16[64,2048]{1,0:T(8,128)(2,1)} %get-tuple-element.4.refs_0_, bf16[128,2048]{1,0:T(8,128)(2,1)} %get-tuple-element.5.refs_1_), custom_call_target="tpu_custom_call" | custom-call | tf_op jit(solution)/shard_map/hand_over/pallas_call | solution.py:603
